TPU v7x, 32 devices: a whole 2x2x4 slice. The times are simulated.
32 devices in a mesh: gr: 2 (over x), fs: 8 (over z, y), tp: 2 (over core).
Axes of the slice: x: 2, y: 2, z: 4, core: 2. Of those that a mesh axis runs over, the one named last changes fastest.
Arguments:
- tokens: bfloat16 [2048, 2048], P(('gr', 'tp')), may hold values from -6 to 6
- norm_gain: float32 [2048], P('fs'), may hold values from 0.1 to 1.9
- up_weight: float32 [2048, 8192], P('fs', ('gr', 'tp')), may hold values from -0.125 to 0.125
- down_weight: float32 [8192, 2048], P('fs', ('gr', 'tp')), may hold values from -0.09375 to 0.09375
Outputs:
- sampler_up: bfloat16 [2048, 8192], P(None, 'fs')
- sampler_down: bfloat16 [8192, 2048], P('fs')
- mixed: bfloat16 [2048, 2048], P(('gr', 'tp'), 'fs')
All inputs are finite; a program needn't handle non-finite values.
Results may differ from a plain program's by a relative error of at most 0.023.
Values may be sent and summed in bfloat16 or wider, within the bound.
A program may use at most 64 MiB of HBM per device.

v0:
```python
import functools

import jax
import jax.numpy as jnp
from jax import lax
from jax.experimental import pallas as pl
from jax.experimental.pallas import tpu as pltpu
from jax.sharding import PartitionSpec as P

MESH = pl.DeviceIdType.MESH
MIB = 1024 * 1024
GATHER_VMEM = 32
PARTIAL_VMEM = 20
REDUCE_VMEM = 20
SLICE_ROWS = 32
PIECES = 2


def flipped(index, step, count):
    if count & (count - 1):
        return lax.rem(index + step, count)
    bit = 1
    while bit < count:
        if step & bit:
            index = index + (1 - 2 * lax.rem(index // bit, 2)) * bit
        bit *= 2
    return index


def remote(src, dst, send, recv, device):
    return pltpu.make_async_remote_copy(
        src_ref=src, dst_ref=dst, send_sem=send, recv_sem=recv,
        device_id=device, device_id_type=MESH,
    )


def gather_kernel(
    tp, blocks, shards, tokens_in, gain_in, up_in, down_in, up_out, down_out, hidden_out,
    tokens, gain, up, down, loads, gath, normed, acc, xs, xr, fsend, frecv, ps, pr, ds_, dr, pds, pdr,
):
    load = [
        pltpu.make_async_copy(source, kept, loads.at[i])
        for i, (source, kept) in enumerate(
            [(gain_in, gain), (up_in, up), (down_in, down), (tokens_in, tokens)]
        )
    ]
    for copy in load:
        copy.start()
    g, f, t = lax.axis_index("gr"), lax.axis_index("fs"), lax.axis_index("tp")
    per = tp // 2
    chips = gath.shape[0]
    c, k = g * per + t // 2, lax.rem(t, 2)
    rows, width = up.shape
    half = rows // 2
    block = width // blocks
    cols = down.shape[1]

    def dev(chip, shard, core):
        return (chip // per, shard, lax.rem(chip, per) * 2 + core)

    def down_cols(chip, core):
        return pl.ds(pl.multiple_of((chip * 2 + core) * cols, cols), cols)

    barrier = pltpu.get_barrier_semaphore()
    for s in range(1, chips):
        pl.semaphore_signal(
            barrier, inc=1, device_id=dev(lax.rem(c + s, chips), f, k), device_id_type=MESH
        )
    for s in range(shards):
        for core in range(2):
            if s == 0 and core == 0:
                continue
            other = lax.rem(f + s, shards)
            core_id = lax.rem(k + core, 2)
            pl.semaphore_signal(
                barrier, inc=1, device_id=dev(c, other, core_id), device_id_type=MESH
            )

    load[0].wait()
    square = (rows, rows)
    diagonal = lax.broadcasted_iota(jnp.int32, square, 0) == lax.broadcasted_iota(jnp.int32, square, 1)
    column = jnp.sum(jnp.where(diagonal, gain[...], 0.0), axis=1, keepdims=True)
    load[1].wait()
    gath[c] = (column * up[...]).astype(jnp.bfloat16)
    load[2].wait()
    down_out[:, down_cols(c, k)] = down[...].astype(jnp.bfloat16)
    pl.semaphore_wait(barrier, chips - 1 + 2 * shards - 1)

    slices = xs.shape[2] // 2
    piece = half // slices

    def unit(chip, j, u):
        return gath.at[chip, pl.ds(u * piece, piece), pl.ds(j * block, block)]

    def up_rows(shard, core):
        return up_out.at[pl.ds(pl.multiple_of(shard * rows + core * half, half), half), :]

    def target(chip, j):
        return (chip * 2 + k) * blocks + j

    def landing(u):
        return up_out.at[pl.ds(pl.multiple_of(f * rows + u * piece, piece), piece), :]

    def forward(chip, j, u):
        to = target(chip, j)
        return remote(
            unit(chip, j, u), landing(u), fsend.at[chip, j, u], frecv.at[f],
            dev(c, to, u // slices),
        )

    def stays(chip, j, u):
        return jnp.logical_and(target(chip, j) == f, k == u // slices)

    def start_forward(chip, j, h):
        @pl.when(jnp.logical_not(stays(chip, j, h)))
        def _():
            forward(chip, j, h).start()

        @pl.when(stays(chip, j, h))
        def _():
            landing(h)[...] = unit(chip, j, h)[...]

    def exchange(s, j, h):
        return remote(
            unit(c, j, h), unit(c, j, h), xs.at[s, j, h], xr.at[s, j, h],
            dev(lax.rem(c + s, chips), f, k),
        )

    def exchanged(s, j, h):
        source = lax.rem(c + chips - s, chips)
        return remote(
            unit(source, j, h), unit(source, j, h), xs.at[s, j, h], xr.at[s, j, h], dev(c, f, k)
        )

    def down_copy(s):
        mine = down_out.at[:, down_cols(c, k)]
        return remote(mine, mine, ds_.at[s], dr.at[s], dev(lax.rem(c + s, chips), f, k))

    def down_relay(s, core):
        held = down_out.at[:, down_cols(lax.rem(c + chips - s, chips), core)]
        return remote(held, held, pds.at[s], pdr.at[s], dev(c, f, 1 - k))

    units = [(j, q + core * slices) for q in range(slices) for core in range(2) for j in range(blocks)]
    for j, h in units:
        for s in range(1, chips):
            exchange(s, j, h).start()
        start_forward(c, j, h)
    for s in range(1, chips):
        down_copy(s).start()
    down_relay(0, k).start()

    load[3].wait()
    widened = tokens[...].astype(jnp.float32)
    scale = lax.rsqrt(jnp.mean(widened * widened, axis=-1, keepdims=True) + 1e-06)
    for shard in range(shards):
        part = tokens[:, shard * rows:(shard + 1) * rows].astype(jnp.float32)
        normed[shard] = (part * scale).astype(jnp.bfloat16)

    for j, h in units:
        for s in range(1, chips):
            exchanged(s, j, h).wait_recv()
            start_forward(lax.rem(c + chips - s, chips), j, h)

    source_core = lax.rem(f // blocks, 2)
    own_stays = source_core == k

    def arrival(shard):
        return remote(
            up_rows(shard, k), up_rows(shard, k), ps.at[shard], frecv.at[shard], dev(c, f, 1 - k)
        )

    def relay(shard, core):
        held = up_rows(shard, core)
        return remote(held, held, ps.at[shard], pr.at[shard], dev(c, f, 1 - k))

    def accumulate(shard, first):
        weights = up_out[pl.ds(pl.multiple_of(shard * rows, rows), rows), :]
        product = jnp.dot(normed[shard], weights, preferred_element_type=jnp.float32)
        if first:
            acc[...] = product
        else:
            acc[...] += product

    order = [flipped(f, s, shards) for s in list(range(1, shards)) + [0]]
    for position, shard in enumerate(order):
        if position < shards - 1:
            arrival(shard).wait_recv()
        else:
            @pl.when(jnp.logical_not(own_stays))
            def _():
                arrival(shard).wait_recv()
        relay(shard, k).start()
        if position > 0:
            before = order[position - 1]
            relay(before, 1 - k).wait_recv()
            accumulate(before, position == 1)
    for s in range(1, chips):
        down_copy_in = remote(
            down_out.at[:, down_cols(lax.rem(c + chips - s, chips), k)],
            down_out.at[:, down_cols(lax.rem(c + chips - s, chips), k)],
            ds_.at[s], dr.at[s], dev(c, f, 1 - k),
        )
        down_copy_in.wait_recv()
        down_relay(s, k).start()
    relay(order[-1], 1 - k).wait_recv()
    accumulate(order[-1], False)
    hidden_out[...] = jnp.square(jnp.maximum(acc[...], 0.0)).astype(jnp.bfloat16)

    for s in range(chips):
        down_relay(s, 1 - k).wait_recv()
        down_relay(s, k).wait_send()
    for s in range(1, chips):
        down_copy(s).wait_send()
        for j, h in units:
            exchange(s, j, h).wait_send()
    for shard in order:
        relay(shard, k).wait_send()
    for s in range(chips):
        chip = lax.rem(c + s, chips)
        for j, h in units:
            @pl.when(jnp.logical_not(stays(chip, j, h)))
            def _():
                forward(chip, j, h).wait_send()


def partial_kernel(hidden, up, down, up_out, down_out, part, sems):
    copies = [
        pltpu.make_async_copy(up, up_out, sems.at[0]),
        pltpu.make_async_copy(down, down_out, sems.at[1]),
    ]
    for copy in copies:
        copy.start()
    shards, _, wide = part.shape
    for pair in range(shards // 2):
        both = jnp.dot(
            hidden[...], down[:, 2 * pair * wide:2 * (pair + 1) * wide],
            preferred_element_type=jnp.float32,
        ).astype(jnp.bfloat16)
        part[2 * pair] = both[:, :wide]
        part[2 * pair + 1] = both[:, wide:]
    for copy in copies:
        copy.wait()


def reduce_kernel(part, mixed, ybuf, zout, zbuf, ys, yr, zs, zr):
    g, f, t = lax.axis_index("gr"), lax.axis_index("fs"), lax.axis_index("tp")
    pairs = ybuf.shape[0]
    wide = mixed.shape[1]
    z, y = f // 2, lax.rem(f, 2)

    barrier = pltpu.get_barrier_semaphore()
    pl.semaphore_signal(
        barrier, inc=1, device_id=(g, z * 2 + 1 - y, t), device_id_type=MESH
    )
    for s in range(1, pairs):
        pl.semaphore_signal(
            barrier, inc=1, device_id=(g, lax.rem(z + s, pairs) * 2 + y, t), device_id_type=MESH
        )
    order = [flipped(z, s, pairs) for s in list(range(pairs - 1, 0, -1)) + [0]]

    pieces = ys.shape[1]
    span = mixed.shape[0] // pieces

    def across(pair, i):
        tokens = pl.ds(i * span, span)
        return remote(
            part.at[2 * pair + 1 - y, tokens], ybuf.at[pair, tokens], ys.at[pair, i],
            yr.at[pair, i], (g, z * 2 + 1 - y, t),
        )

    def along(pair, sender, i):
        tokens = pl.ds(i * span, span)
        return remote(
            zout.at[pair, tokens], zbuf.at[sender, tokens], zs.at[pair, i], zr.at[sender, i],
            (g, pair * 2 + y, t),
        )

    pl.semaphore_wait(barrier, pairs)
    for pair in order:
        for i in range(pieces):
            across(pair, i).start()

    def summed(pair, i):
        tokens = pl.ds(i * span, span)
        return part[2 * pair + y, tokens].astype(jnp.float32) + ybuf[pair, tokens].astype(jnp.float32)

    for pair in order[:-1]:
        for i in range(pieces):
            across(pair, i).wait_recv()
            zout[pair, pl.ds(i * span, span)] = summed(pair, i).astype(jnp.bfloat16)
            along(pair, z, i).start()
    for i in range(pieces):
        tokens = pl.ds(i * span, span)
        across(z, i).wait_recv()
        total = summed(z, i)
        for pair in order[:-1]:
            along(z, pair, i).wait_recv()
            total = total + zbuf[pair, tokens].astype(jnp.float32)
        mixed[tokens] = total.astype(jnp.bfloat16)
    for i in range(pieces):
        for pair in order:
            across(pair, i).wait_send()
        for pair in order[:-1]:
            along(pair, z, i).wait_send()


def per_device(gr, fs, tp, tokens, norm_gain, up_weight, down_weight):
    rows, width = up_weight.shape
    units, cols = down_weight.shape
    group = gr * tp
    chips = group // 2
    slices = max(1, rows // 2 // SLICE_ROWS)
    block = width * group // fs
    blocks = width // block
    count, depth = tokens.shape
    model = cols * group
    vmem = pl.BlockSpec(memory_space=pltpu.VMEM)
    hbm = pl.BlockSpec(memory_space=pltpu.HBM)
    bf16, f32 = jnp.bfloat16, jnp.float32
    dma = pltpu.SemaphoreType.DMA
    up_block, down_columns, hidden = pl.pallas_call(
        functools.partial(gather_kernel, tp, blocks, fs),
        out_shape=(
            jax.ShapeDtypeStruct((depth, block), bf16),
            jax.ShapeDtypeStruct((units, model), bf16),
            jax.ShapeDtypeStruct((count, block), bf16),
        ),
        in_specs=[hbm] * 4,
        out_specs=(vmem,) * 3,
        scratch_shapes=[
            pltpu.VMEM(tokens.shape, bf16),
            pltpu.VMEM((1, rows), f32),
            pltpu.VMEM(up_weight.shape, f32),
            pltpu.VMEM(down_weight.shape, f32),
            dma((4,)),
            pltpu.VMEM((chips, rows, width), bf16),
            pltpu.VMEM((fs, count, rows), bf16),
            pltpu.VMEM((count, block), f32),
            *[dma((chips, blocks, 2 * slices)) for _ in range(3)], dma((fs,)),
            dma((fs,)), dma((fs,)),
            dma((chips,)), dma((chips,)), dma((chips,)), dma((chips,)),
        ],
        compiler_params=pltpu.CompilerParams(
            collective_id=0, has_side_effects=True, vmem_limit_bytes=GATHER_VMEM * MIB
        ),
        cost_estimate=pl.CostEstimate(
            flops=2 * count * depth * block, bytes_accessed=160 * MIB, transcendentals=0
        ),
    )(*[pltpu.with_memory_space_constraint(x, pltpu.HBM) for x in (tokens, norm_gain[None, :], up_weight, down_weight)])
    pairs = fs // 2
    wide = model // fs
    up_block, down_columns, part = pl.pallas_call(
        partial_kernel,
        out_shape=(
            jax.ShapeDtypeStruct(up_block.shape, bf16),
            jax.ShapeDtypeStruct(down_columns.shape, bf16),
            jax.ShapeDtypeStruct((fs, count, wide), bf16),
        ),
        in_specs=[vmem] * 3,
        out_specs=(hbm, hbm, vmem),
        scratch_shapes=[dma((2,))],
        compiler_params=pltpu.CompilerParams(vmem_limit_bytes=PARTIAL_VMEM * MIB),
        cost_estimate=pl.CostEstimate(
            flops=2 * count * units * model, bytes_accessed=16 * MIB, transcendentals=0
        ),
    )(hidden, up_block, down_columns)
    mixed = pl.pallas_call(
        reduce_kernel,
        out_shape=jax.ShapeDtypeStruct((count, wide), bf16),
        in_specs=[vmem],
        out_specs=vmem,
        scratch_shapes=[
            pltpu.VMEM((pairs, count, wide), bf16),
            pltpu.VMEM((pairs, count, wide), bf16),
            pltpu.VMEM((pairs, count, wide), bf16),
            *[dma((pairs, PIECES)) for _ in range(4)],
        ],
        compiler_params=pltpu.CompilerParams(
            collective_id=1, has_side_effects=True, vmem_limit_bytes=REDUCE_VMEM * MIB
        ),
        cost_estimate=pl.CostEstimate(
            flops=count * model, bytes_accessed=100 * MIB, transcendentals=0
        ),
    )(part)
    return (up_block, down_columns, mixed)


def solution(mesh):
    in_specs = (P(("gr", "tp"), None), P("fs"), P("fs", ("gr", "tp")), P("fs", ("gr", "tp")))
    out_specs = (P(None, "fs"), P("fs", None), P(("gr", "tp"), "fs"))
    body = functools.partial(per_device, mesh.shape["gr"], mesh.shape["fs"], mesh.shape["tp"])
    return jax.shard_map(
        body, mesh=mesh, in_specs=in_specs, out_specs=out_specs, check_vma=False
    )
```

profile of v0, /device:TPU:0, one launch (start us, length us, event | category | flops | bytes accessed | tf_op | source)
XLA Modules:
  0.0 98.8 jit_solution(10885051095141170184)
XLA Ops:
  0.6 58.8 %shard_map.67 = (bf16[2048,1024]{1,0:T(8,128)(2,1)S(1)}, bf16[1024,2048]{1,0:T(8,128)(2,1)S(1)}, bf16[512,1024]{1,0:T(8,128)(2,1)S(1)}) custom-call(bf16[512,2048]{1,0:T(8,128)(2,1)} %tokens_in.1, f32[1,256]{1,0:T(1,128)} %bitcast.1, f32[256,2048]{1,0:T(8,128)} %up_in.1, f32[1024,512]{1,0:T(8,128)} %down_in.1), custom_call_target="tpu_custom_call" | custom-call | flops 2147483648 | bytes 167772160 | tf_op jit(solution)/shard_map/pallas_call | solution.py:321
  59.4 3.4 %shard_map.68 = (bf16[2048,1024]{1,0:T(8,128)(2,1)}, bf16[1024,2048]{1,0:T(8,128)(2,1)}, bf16[8,512,256]{2,1,0:T(8,128)(2,1)S(1)}) custom-call(bf16[512,1024]{1,0:T(8,128)(2,1)S(1)} %get-tuple-element.9.hidden, bf16[2048,1024]{1,0:T(8,128)(2,1)S(1)} %get-tuple-element.10.up, bf16[1024,2048]{1,0:T(8,128)(2,1)S(1)} %get-tuple-element.11.down), custom_call_target="tpu_custom_call" | custom-call | flops 2147483648 | bytes 16777216 | tf_op jit(solution)/shard_map/pallas_call | solution.py:352
  62.8 35.2 %shard_map.69 = bf16[512,256]{1,0:T(8,128)(2,1)S(1)} custom-call(bf16[8,512,256]{2,1,0:T(8,128)(2,1)S(1)} %get-tuple-element.14.part), custom_call_target="tpu_custom_call" | custom-call | flops 1048576 | bytes 104857600 | tf_op jit(solution)/shard_map/pallas_call | solution.py:367
  98.1 0.7 copy.8
where the time goes:
time: 98.9 us; the launch traced here: 98.8 us
  Pallas kernels  97.4 us (98%)
    pallas_call x1, Pallas kernels, per_device(): pl.pallas_call(functools.partial(gather_kernel, tp, blocks, fs), out_shap...  58.8 us
    pallas_call x1, Pallas kernels, per_device(): pl.pallas_call(reduce_kernel, out_shape=jax.ShapeDtypeStruct((count, wide...  35.2 us
    pallas_call x1, Pallas kernels, per_device(): pl.pallas_call(partial_kernel, out_shape=(jax.ShapeDtypeStruct(up_block.s...  3.41 us

commit v1 on v0

v1 whole, which is shorter than its diff:
```python
import functools

import jax
import jax.numpy as jnp
from jax import lax
from jax.experimental import pallas as pl
from jax.experimental.pallas import tpu as pltpu
from jax.sharding import PartitionSpec as P

MESH = pl.DeviceIdType.MESH
MIB = 1024 * 1024
FUSED_VMEM = 36
COPY_VMEM = 4
SLICE_ROWS = 32
SINGLE_NUM, SINGLE_DEN = 1, 4
PIECES = 4
DOWN_CHUNKS = 2
COPY_CHUNKS = 4


def flipped(index, step, count):
    if count & (count - 1):
        return lax.rem(index + step, count)
    bit = 1
    while bit < count:
        if step & bit:
            index = index + (1 - 2 * lax.rem(index // bit, 2)) * bit
        bit *= 2
    return index


def remote(src, dst, send, recv, device):
    return pltpu.make_async_remote_copy(
        src_ref=src, dst_ref=dst, send_sem=send, recv_sem=recv,
        device_id=device, device_id_type=MESH,
    )


def when_not(condition):
    return pl.when(jnp.logical_not(condition))


def fused_kernel(
    tp, blocks, shards, single, tokens_in, gain_in, up_in, down_in, up_out, down_out, mixed,
    tokens, gain, up, down, loads, gath, normed, acc, hidden, part, ybuf, zout, zin,
    xs, xr, fsend, frecv, msend, ps, pr, ods, odr, xds, xdr, pds, pdr, ys, yr, zs, zr,
):
    load = [
        pltpu.make_async_copy(source, kept, loads.at[i])
        for i, (source, kept) in enumerate(
            [(gain_in, gain), (up_in, up), (down_in, down), (tokens_in, tokens)]
        )
    ]
    for copy in load:
        copy.start()
    g, f, t = lax.axis_index("gr"), lax.axis_index("fs"), lax.axis_index("tp")
    per = tp // 2
    chips = gath.shape[0]
    c, k = g * per + t // 2, lax.rem(t, 2)
    rows, width = up.shape
    half = rows // 2
    block = width // blocks
    cols = down.shape[1]
    pairs = ybuf.shape[0]
    wide = mixed.shape[1]
    z, y = f // 2, lax.rem(f, 2)

    def dev(chip, shard, core):
        return (chip // per, shard, lax.rem(chip, per) * 2 + core)

    def down_cols(pair):
        return pl.ds(pl.multiple_of(pair * cols, cols), cols)

    barrier = pltpu.get_barrier_semaphore()
    for s in range(1, chips):
        pl.semaphore_signal(
            barrier, inc=1, device_id=dev(lax.rem(c + s, chips), f, k), device_id_type=MESH
        )
    for s in range(shards):
        for core in range(2):
            if s == 0 and core == 0:
                continue
            other = lax.rem(f + s, shards)
            core_id = lax.rem(k + core, 2)
            pl.semaphore_signal(
                barrier, inc=1, device_id=dev(c, other, core_id), device_id_type=MESH
            )

    load[0].wait()
    square = (rows, rows)
    diagonal = lax.broadcasted_iota(jnp.int32, square, 0) == lax.broadcasted_iota(jnp.int32, square, 1)
    column = jnp.sum(jnp.where(diagonal, gain[...], 0.0), axis=1, keepdims=True)
    load[1].wait()
    gath[c] = (column * up[...]).astype(jnp.bfloat16)
    pl.semaphore_wait(barrier, chips - 1 + 2 * shards - 1)

    slices = xs.shape[2] // 2
    piece = half // slices

    def route(u):
        q = u % slices
        return 1 if q < single else 0 if q < 2 * single else None

    def crosses(source, target):
        return source // (shards // 2) != target // (shards // 2)

    def unit(chip, j, u):
        return gath.at[chip, pl.ds(u * piece, piece), pl.ds(j * block, block)]

    def half_rows(shard, core, first=0, count=half):
        at = pl.multiple_of(shard * rows + core * half + first, piece)
        return up_out.at[pl.ds(at, count), :]

    def target(chip, j):
        return (chip * 2 + k) * blocks + j

    def landing(u):
        return up_out.at[pl.ds(pl.multiple_of(f * rows + u * piece, piece), piece), :]

    def stays(chip, j, u):
        return jnp.logical_and(target(chip, j) == f, k == u // slices)

    def forward(chip, j, u):
        to = target(chip, j)
        at = f if route(u) is None else f + jnp.where(crosses(f, to), shards, 0)
        return remote(
            unit(chip, j, u), landing(u), fsend.at[chip, j, u], frecv.at[at], dev(c, to, u // slices)
        )

    def start_forward(chip, j, u):
        @when_not(stays(chip, j, u))
        def _():
            forward(chip, j, u).start()

        @pl.when(stays(chip, j, u))
        def _():
            landing(u)[...] = unit(chip, j, u)[...]

    def goes(chip, j, u, offset, action):
        if route(u) is None or route(u) == offset:
            action()
        else:
            when_not(crosses(f, target(chip, j)))(action)

    def exchange(s, j, u):
        return remote(
            unit(c, j, u), unit(c, j, u), xs.at[s, j, u], xr.at[s, j, u],
            dev(lax.rem(c + s, chips), f, k),
        )

    def exchanged(s, j, u):
        source = lax.rem(c + chips - s, chips)
        return remote(
            unit(source, j, u), unit(source, j, u), xs.at[s, j, u], xr.at[s, j, u], dev(c, f, k)
        )

    units = [
        [(j, q + core * slices) for core in range(2) for j in range(blocks)] for q in range(slices)
    ]
    for group in units:
        for j, u in group:
            for s in range(1, chips):
                goes(c, j, u, s, lambda: exchange(s, j, u).start())
            goes(c, j, u, 0, lambda: start_forward(c, j, u))

    load[2].wait()
    own_pair = c * 2 + k
    down_out[:, down_cols(own_pair)] = down[...].astype(jnp.bfloat16)
    down_half = down.shape[0] // 2
    chunks = xds.shape[2]
    chunk = down_half // chunks

    def down_own(core):
        held = down_out.at[:, down_cols(c * 2 + core)]
        return remote(held, held, ods.at[0], odr.at[0], dev(c, f, 1 - k))

    down_own(k).start()

    def pair_of(chip, position):
        low = 2 * chip
        return low + jnp.where(z <= low, 1 - position, position)

    def down_piece(pair, core, i):
        at = pl.multiple_of(core * down_half + i * chunk, chunk)
        return down_out.at[pl.ds(at, chunk), down_cols(pair)]

    def down_across(s, position, i):
        held = down_piece(pair_of(c, position), k, i)
        return remote(
            held, held, xds.at[s, position, i], xdr.at[s, position, i],
            dev(lax.rem(c + s, chips), f, k),
        )

    def down_relay(s, position, i, core):
        held = down_piece(pair_of(lax.rem(c + chips - s, chips), position), core, i)
        return remote(held, held, pds.at[s, position, i], pdr.at[s, position, i], dev(c, f, 1 - k))

    def down_arrival(s, position, i):
        held = down_piece(pair_of(lax.rem(c + chips - s, chips), position), k, i)
        return remote(held, held, xds.at[s, position, i], xdr.at[s, position, i], dev(c, f, k))

    load[3].wait()
    widened = tokens[...].astype(jnp.float32)
    scale = lax.rsqrt(jnp.mean(widened * widened, axis=-1, keepdims=True) + 1e-06)
    for shard in range(shards):
        share = tokens[:, shard * rows:(shard + 1) * rows].astype(jnp.float32)
        normed[shard] = (share * scale).astype(jnp.bfloat16)

    owner = f // (2 * blocks)
    offset = lax.rem(c + chips - owner, chips)
    lone = single * piece

    def alone(shard):
        return jnp.logical_and(crosses(shard, f), offset < 2)

    def lone_rows(shard):
        return half_rows(shard, k, (1 - offset) * lone, lone)

    def lone_arrival(shard):
        return remote(
            lone_rows(shard), lone_rows(shard), msend.at[shard, 0], frecv.at[shards + shard], dev(c, f, k)
        )

    def lone_relay(shard, s):
        return remote(
            lone_rows(shard), lone_rows(shard), msend.at[shard, s], frecv.at[shard],
            dev(lax.rem(c + s, chips), f, k),
        )

    even = not shards & (shards - 1)
    far = [s for s in range(1, shards) if single and (not even or s & (shards // 2))]

    def relay_lone():
        for step in far:
            shard = flipped(f, step, shards)

            @pl.when(alone(shard))
            def _():
                lone_arrival(shard).wait_recv()
                for s in range(1, chips):
                    lone_relay(shard, s).start()

    def send_down():
        down_own(1 - k).wait_recv()
        for position in range(2):
            for i in range(chunks):
                for s in range(1, chips):
                    down_across(s, position, i).start()

    for q, group in enumerate(units):
        if q == max(0, slices - 1):
            relay_lone()
            send_down()
        for j, u in group:
            for s in range(1, chips):
                source = lax.rem(c + chips - s, chips)

                def pass_on():
                    exchanged(s, j, u).wait_recv()
                    start_forward(source, j, u)

                goes(source, j, u, s, pass_on)

    source_core = lax.rem(f // blocks, 2)
    own_stays = source_core == k

    def arrive(shard, step):
        def arrival(count):
            held = half_rows(shard, k, 0, count)
            return remote(held, held, ps.at[shard], frecv.at[shard], dev(c, f, 1 - k))

        if step in far:
            @pl.when(alone(shard))
            def _():
                arrival(half - lone).wait_recv()

            @when_not(alone(shard))
            def _():
                arrival(half).wait_recv()
        elif step == 0:
            @when_not(own_stays)
            def _():
                arrival(half).wait_recv()
        else:
            arrival(half).wait_recv()

    def relay(shard, core):
        held = half_rows(shard, core)
        return remote(held, held, ps.at[shard], pr.at[shard], dev(c, f, 1 - k))

    def accumulate(shard, first):
        weights = up_out[pl.ds(pl.multiple_of(shard * rows, rows), rows), :]
        product = jnp.dot(normed[shard], weights, preferred_element_type=jnp.float32)
        if first:
            acc[...] = product
        else:
            acc[...] += product

    near = shards // 2
    steps = list(range(1, near)) + [0] + list(range(near, shards))
    order = [flipped(f, s, shards) for s in steps]
    for position, shard in enumerate(order):
        arrive(shard, steps[position])
        relay(shard, k).start()
        if position > 0:
            before = order[position - 1]
            relay(before, 1 - k).wait_recv()
            accumulate(before, position == 1)
    relay(order[-1], 1 - k).wait_recv()
    accumulate(order[-1], False)
    hidden[...] = jnp.square(jnp.maximum(acc[...], 0.0)).astype(jnp.bfloat16)

    pieces = ys.shape[1]
    span = mixed.shape[0] // pieces

    def across(pair, i):
        at = pl.ds(i * span, span)
        return remote(
            part.at[2 * pair + 1 - y, at], ybuf.at[pair, at], ys.at[pair, i], yr.at[pair, i],
            dev(c, z * 2 + 1 - y, k),
        )

    def along(pair, i):
        at = pl.ds(i * span, span)
        to = z + jnp.where(pair > z, 1, -1)
        slot = jnp.where(jnp.logical_and(pair < z, pair == to), pairs, pair)
        return remote(
            zout.at[pair, at], zin.at[slot, at], zs.at[pair, i], zr.at[slot, i], dev(c, to * 2 + y, k)
        )

    def carried(slot, i):
        held = zin.at[slot, pl.ds(i * span, span)]
        return remote(held, held, zs.at[0, i], zr.at[slot, i], dev(c, f, k))

    def multiply(pair):
        both = jnp.dot(
            hidden[...], down_out[:, down_cols(pair)], preferred_element_type=jnp.float32
        ).astype(jnp.bfloat16)
        part[2 * pair] = both[:, :wide]
        part[2 * pair + 1] = both[:, wide:]
        for i in range(pieces):
            across(pair, i).start()

    def reduce(pair):
        inner = jnp.logical_and(pair != z, jnp.where(pair > z, z > 0, z < pairs - 1))
        outer = jnp.logical_and(pair != z, jnp.logical_not(inner))
        for i in range(pieces):
            at = pl.ds(i * span, span)

            def wide_of(ref, slot):
                return ref[slot, at].astype(jnp.float32)

            def summed():
                return wide_of(part, 2 * pair + y) + wide_of(ybuf, pair)

            across(pair, i).wait_recv()

            @pl.when(inner)
            def _():
                carried(pair, i).wait_recv()
                zout[pair, at] = (summed() + wide_of(zin, pair)).astype(jnp.bfloat16)
                along(pair, i).start()

            @pl.when(outer)
            def _():
                zout[pair, at] = summed().astype(jnp.bfloat16)
                along(pair, i).start()

            @pl.when(pair == z)
            def _():
                @pl.when(z == 0)
                def _():
                    carried(pairs, i).wait_recv()
                    mixed[at] = (summed() + wide_of(zin, pairs)).astype(jnp.bfloat16)

                @pl.when(z == pairs - 1)
                def _():
                    carried(pair, i).wait_recv()
                    mixed[at] = (summed() + wide_of(zin, pair)).astype(jnp.bfloat16)

                @pl.when(jnp.logical_and(z > 0, z < pairs - 1))
                def _():
                    carried(pair, i).wait_recv()
                    carried(pairs, i).wait_recv()
                    total = summed() + wide_of(zin, pair) + wide_of(zin, pairs)
                    mixed[at] = total.astype(jnp.bfloat16)

    def fetch(s, position):
        for i in range(chunks):
            down_arrival(s, position, i).wait_recv()
            down_relay(s, position, i, k).start()
        for i in range(chunks):
            down_relay(s, position, i, 1 - k).wait_recv()

    sequence = [
        (s, position, pair_of(lax.rem(c + chips - s, chips), position))
        for s in range(chips) for position in range(2)
    ]
    ahead = 3
    for i, (s, position, pair) in enumerate(sequence):
        if s > 0:
            fetch(s, position)
        multiply(pair)
        if i >= ahead - 1:
            reduce(sequence[i - ahead + 1][2])
    for _, _, pair in sequence[len(sequence) - ahead + 1:]:
        reduce(pair)

    down_own(k).wait_send()
    for s in range(1, chips):
        for position in range(2):
            for i in range(chunks):
                down_across(s, position, i).wait_send()
                down_relay(s, position, i, k).wait_send()
    for step in far:
        shard = flipped(f, step, shards)

        @pl.when(alone(shard))
        def _():
            for s in range(1, chips):
                lone_relay(shard, s).wait_send()
    for group in units:
        for j, u in group:
            for s in range(1, chips):
                goes(c, j, u, s, lambda: exchange(s, j, u).wait_send())
            for s in range(chips):
                source = lax.rem(c + chips - s, chips)

                def sent():
                    @when_not(stays(source, j, u))
                    def _():
                        forward(source, j, u).wait_send()

                goes(source, j, u, s, sent)
    for shard in order:
        relay(shard, k).wait_send()
    for _, _, pair in sequence:
        for i in range(pieces):
            across(pair, i).wait_send()

            @pl.when(pair != z)
            def _():
                along(pair, i).wait_send()


def copy_kernel(up, down, mixed, up_out, down_out, mixed_out, sems):
    copies = []
    for index, (source, kept) in enumerate([(up, up_out), (down, down_out), (mixed, mixed_out)]):
        count = sems.shape[1]
        span = source.shape[0] // count
        for i in range(count):
            at = pl.ds(i * span, span)
            copies.append(pltpu.make_async_copy(source.at[at], kept.at[at], sems.at[index, i]))
    for copy in copies:
        copy.start()
    for copy in copies:
        copy.wait()


def per_device(gr, fs, tp, tokens, norm_gain, up_weight, down_weight):
    rows, width = up_weight.shape
    units, cols = down_weight.shape
    group = gr * tp
    chips = group // 2
    slices = max(1, rows // 2 // SLICE_ROWS)
    single = slices * SINGLE_NUM // SINGLE_DEN if chips > 1 else 0
    block = width * group // fs
    blocks = width // block
    count, depth = tokens.shape
    model = cols * group
    pairs = fs // 2
    wide = model // fs
    assert pairs == group and pairs > 1
    vmem = pl.BlockSpec(memory_space=pltpu.VMEM)
    hbm = pl.BlockSpec(memory_space=pltpu.HBM)
    bf16, f32 = jnp.bfloat16, jnp.float32
    dma = pltpu.SemaphoreType.DMA
    results = (
        jax.ShapeDtypeStruct((depth, block), bf16),
        jax.ShapeDtypeStruct((units, model), bf16),
        jax.ShapeDtypeStruct((count, wide), bf16),
    )
    arrays = pl.pallas_call(
        functools.partial(fused_kernel, tp, blocks, fs, single),
        out_shape=results,
        in_specs=[hbm] * 4,
        out_specs=(vmem,) * 3,
        scratch_shapes=[
            pltpu.VMEM(tokens.shape, bf16),
            pltpu.VMEM((1, rows), f32),
            pltpu.VMEM(up_weight.shape, f32),
            pltpu.VMEM(down_weight.shape, f32),
            dma((4,)),
            pltpu.VMEM((chips, rows, width), bf16),
            pltpu.VMEM((fs, count, rows), bf16),
            pltpu.VMEM((count, block), f32),
            pltpu.VMEM((count, block), bf16),
            pltpu.VMEM((fs, count, wide), bf16),
            pltpu.VMEM((pairs, count, wide), bf16),
            pltpu.VMEM((pairs, count, wide), bf16),
            pltpu.VMEM((pairs + 1, count, wide), bf16),
            *[dma((chips, blocks, 2 * slices)) for _ in range(3)], dma((2 * fs,)), dma((fs, chips)),
            dma((fs,)), dma((fs,)), dma((1,)), dma((1,)),
            *[dma((chips, 2, DOWN_CHUNKS)) for _ in range(4)],
            *[dma((pairs, PIECES)) for _ in range(3)], dma((pairs + 1, PIECES)),
        ],
        compiler_params=pltpu.CompilerParams(
            collective_id=0, has_side_effects=True, vmem_limit_bytes=FUSED_VMEM * MIB
        ),
        cost_estimate=pl.CostEstimate(
            flops=2 * count * block * (depth + model), bytes_accessed=160 * MIB, transcendentals=0
        ),
    )(*[pltpu.with_memory_space_constraint(x, pltpu.HBM) for x in (tokens, norm_gain[None, :], up_weight, down_weight)])
    return pl.pallas_call(
        copy_kernel,
        out_shape=results,
        in_specs=[vmem] * 3,
        out_specs=(hbm,) * 3,
        scratch_shapes=[dma((3, COPY_CHUNKS))],
        compiler_params=pltpu.CompilerParams(vmem_limit_bytes=COPY_VMEM * MIB),
        cost_estimate=pl.CostEstimate(flops=count * wide, bytes_accessed=18 * MIB, transcendentals=0),
    )(*arrays)


def solution(mesh):
    in_specs = (P(("gr", "tp"), None), P("fs"), P("fs", ("gr", "tp")), P("fs", ("gr", "tp")))
    out_specs = (P(None, "fs"), P("fs", None), P(("gr", "tp"), "fs"))
    body = functools.partial(per_device, mesh.shape["gr"], mesh.shape["fs"], mesh.shape["tp"])
    return jax.shard_map(
        body, mesh=mesh, in_specs=in_specs, out_specs=out_specs, check_vma=False
    )
```

time: 98.9 us -> 88.7 us (0.90)
  the two profiles are of different devices: /device:TPU:0 before, /device:TPU:10 now
where the time goes in v1:
time: 88.7 us; the launch traced here: 88.6 us
  Pallas kernels  87.9 us (99%)
    pallas_call x1, Pallas kernels, per_device(): pl.pallas_call(functools.partial(fused_kernel, tp, blocks, fs, single), o...  84.5 us
    pallas_call x1, Pallas kernels, per_device(): pl.pallas_call(copy_kernel, out_shape=results, in_specs=[vmem] * 3, out_s...  3.44 us

profile of v1, /device:TPU:10, one launch (start us, length us, event | category | flops | bytes accessed | tf_op | source)
XLA Modules:
  0.0 88.6 jit_solution(6670748809195128893)
XLA Ops:
  0.6 84.5 %shard_map.67 = (bf16[2048,1024]{1,0:T(8,128)(2,1)S(1)}, bf16[1024,2048]{1,0:T(8,128)(2,1)S(1)}, bf16[512,256]{1,0:T(8,128)(2,1)S(1)}) custom-call(bf16[512,2048]{1,0:T(8,128)(2,1)} %tokens_in.1, f32[1,256]{1,0:T(1,128)} %bitcast.1, f32[256,2048]{1,0:T(8,128)} %up_in.1, f32[1024,512]{1,0:T(8,128)} %down_in.1), custom_call_target="tpu_custom_call" | custom-call | flops 4294967296 | bytes 167772160 | tf_op jit(solution)/shard_map/pallas_call | solution.py:483
  85.1 3.4 %shard_map.68 = (bf16[2048,1024]{1,0:T(8,128)(2,1)}, bf16[1024,2048]{1,0:T(8,128)(2,1)}, bf16[512,256]{1,0:T(8,128)(2,1)}) custom-call(bf16[2048,1024]{1,0:T(8,128)(2,1)S(1)} %get-tuple-element.6.up, bf16[1024,2048]{1,0:T(8,128)(2,1)S(1)} %get-tuple-element.7.down, bf16[512,256]{1,0:T(8,128)(2,1)S(1)} %get-tuple-element.8.mixed), custom_call_target="tpu_custom_call" | custom-call | flops 131072 | bytes 18874368 | tf_op jit(solution)/shard_map/pallas_call | solution.py:514

commit v2 on v1

--- a/solution.py
+++ b/solution.py
@@ -16,6 +16,7 @@
 PIECES = 4
 DOWN_CHUNKS = 2
 COPY_CHUNKS = 4
+AHEAD = 2
 
 
 def flipped(index, step, count):
@@ -161,7 +162,8 @@
         for j, u in group:
             for s in range(1, chips):
                 goes(c, j, u, s, lambda: exchange(s, j, u).start())
-            goes(c, j, u, 0, lambda: start_forward(c, j, u))
+            if route(u) in (None, 0):
+                pl.when(crosses(f, target(c, j)))(lambda: forward(c, j, u).start())
 
     load[2].wait()
     own_pair = c * 2 + k
@@ -248,10 +250,8 @@
                     down_across(s, position, i).start()
 
     for q, group in enumerate(units):
-        if q == max(0, slices - 1):
-            relay_lone()
-            send_down()
         for j, u in group:
+            when_not(crosses(f, target(c, j)))(lambda: start_forward(c, j, u))
             for s in range(1, chips):
                 source = lax.rem(c + chips - s, chips)
 
@@ -260,6 +260,8 @@
                     start_forward(source, j, u)
 
                 goes(source, j, u, s, pass_on)
+    relay_lone()
+    send_down()
 
     source_core = lax.rem(f // blocks, 2)
     own_stays = source_core == k
@@ -392,18 +394,18 @@
         for i in range(chunks):
             down_relay(s, position, i, 1 - k).wait_recv()
 
-    sequence = [
-        (s, position, pair_of(lax.rem(c + chips - s, chips), position))
-        for s in range(chips) for position in range(2)
-    ]
-    ahead = 3
-    for i, (s, position, pair) in enumerate(sequence):
-        if s > 0:
-            fetch(s, position)
-        multiply(pair)
-        if i >= ahead - 1:
-            reduce(sequence[i - ahead + 1][2])
-    for _, _, pair in sequence[len(sequence) - ahead + 1:]:
+    def pair_at(index):
+        return pair_of(lax.rem(c + chips - index // 2, chips), lax.rem(index, 2))
+
+    last = 2 * lax.rem(z // 2 + chips - c, chips) + 1
+    sequence = [pair_at(i + jnp.where(i < last, 0, 1)) for i in range(pairs - 1)] + [pair_at(last)]
+    for i in range(pairs):
+        if i > 1:
+            fetch(i // 2, i % 2)
+        multiply(pair_at(i))
+        if i >= AHEAD:
+            reduce(sequence[i - AHEAD])
+    for pair in sequence[pairs - AHEAD:]:
         reduce(pair)
 
     down_own(k).wait_send()
@@ -434,7 +436,7 @@
                 goes(source, j, u, s, sent)
     for shard in order:
         relay(shard, k).wait_send()
-    for _, _, pair in sequence:
+    for pair in sequence:
         for i in range(pieces):
             across(pair, i).wait_send()
 

time: 88.7 us -> 82.8 us (0.933)
  Pallas kernels: 87.9 us -> 81.7 us
    pallas_call x1, Pallas kernels: 84.5 us -> 78.2 us  [per_device(): pl.pallas_call(functools.partial(fused_kernel, tp, blocks, fs, single), o...]
where the time goes in v2:
time: 82.8 us; the launch traced here: 82.3 us
  Pallas kernels  81.7 us (99%)
    pallas_call x1, Pallas kernels, per_device(): pl.pallas_call(functools.partial(fused_kernel, tp, blocks, fs, single), o...  78.2 us
    pallas_call x1, Pallas kernels, per_device(): pl.pallas_call(copy_kernel, out_shape=results, in_specs=[vmem] * 3, out_s...  3.44 us

profile of v2, /device:TPU:10, one launch (start us, length us, event | category | flops | bytes accessed | tf_op | source)
XLA Modules:
  0.0 82.3 jit_solution(18235431397376371681)
XLA Ops:
  0.6 78.2 %shard_map.67 = (bf16[2048,1024]{1,0:T(8,128)(2,1)S(1)}, bf16[1024,2048]{1,0:T(8,128)(2,1)S(1)}, bf16[512,256]{1,0:T(8,128)(2,1)S(1)}) custom-call(bf16[512,2048]{1,0:T(8,128)(2,1)} %tokens_in.1, f32[1,256]{1,0:T(1,128)} %bitcast.1, f32[256,2048]{1,0:T(8,128)} %up_in.1, f32[1024,512]{1,0:T(8,128)} %down_in.1), custom_call_target="tpu_custom_call" | custom-call | flops 4294967296 | bytes 167772160 | tf_op jit(solution)/shard_map/pallas_call | solution.py:485
  78.9 3.4 %shard_map.68 = (bf16[2048,1024]{1,0:T(8,128)(2,1)}, bf16[1024,2048]{1,0:T(8,128)(2,1)}, bf16[512,256]{1,0:T(8,128)(2,1)}) custom-call(bf16[2048,1024]{1,0:T(8,128)(2,1)S(1)} %get-tuple-element.6.up, bf16[1024,2048]{1,0:T(8,128)(2,1)S(1)} %get-tuple-element.7.down, bf16[512,256]{1,0:T(8,128)(2,1)S(1)} %get-tuple-element.8.mixed), custom_call_target="tpu_custom_call" | custom-call | flops 131072 | bytes 18874368 | tf_op jit(solution)/shard_map/pallas_call | solution.py:516

commit v3 on v2

--- a/solution.py
+++ b/solution.py
@@ -12,11 +12,10 @@
 FUSED_VMEM = 36
 COPY_VMEM = 4
 SLICE_ROWS = 32
-SINGLE_NUM, SINGLE_DEN = 1, 4
+SINGLE = ((1, 4), (1, 4))
 PIECES = 4
 DOWN_CHUNKS = 2
-COPY_CHUNKS = 4
-AHEAD = 2
+COPY_CHUNKS = 2
 
 
 def flipped(index, step, count):
@@ -95,12 +94,12 @@
     gath[c] = (column * up[...]).astype(jnp.bfloat16)
     pl.semaphore_wait(barrier, chips - 1 + 2 * shards - 1)
 
-    slices = xs.shape[2] // 2
+    slices = xr.shape[2] // 2
     piece = half // slices
 
     def route(u):
         q = u % slices
-        return 1 if q < single else 0 if q < 2 * single else None
+        return 1 if q < single[1] else 0 if q < sum(single) else None
 
     def crosses(source, target):
         return source // (shards // 2) != target // (shards // 2)
@@ -121,17 +120,21 @@
     def stays(chip, j, u):
         return jnp.logical_and(target(chip, j) == f, k == u // slices)
 
-    def forward(chip, j, u):
+    def pinned(u, s):
+        return 0 if route(u) in (None, s) else 1
+
+    def forward(chip, j, u, s):
         to = target(chip, j)
         at = f if route(u) is None else f + jnp.where(crosses(f, to), shards, 0)
         return remote(
-            unit(chip, j, u), landing(u), fsend.at[chip, j, u], frecv.at[at], dev(c, to, u // slices)
-        )
-
-    def start_forward(chip, j, u):
+            unit(chip, j, u), landing(u), fsend.at[s, j, pinned(u, s)], frecv.at[at],
+            dev(c, to, u // slices),
+        )
+
+    def start_forward(chip, j, u, s):
         @when_not(stays(chip, j, u))
         def _():
-            forward(chip, j, u).start()
+            forward(chip, j, u, s).start()
 
         @pl.when(stays(chip, j, u))
         def _():
@@ -145,14 +148,14 @@
 
     def exchange(s, j, u):
         return remote(
-            unit(c, j, u), unit(c, j, u), xs.at[s, j, u], xr.at[s, j, u],
+            unit(c, j, u), unit(c, j, u), xs.at[s - 1, pinned(u, s)], xr.at[s - 1, j, u],
             dev(lax.rem(c + s, chips), f, k),
         )
 
     def exchanged(s, j, u):
         source = lax.rem(c + chips - s, chips)
         return remote(
-            unit(source, j, u), unit(source, j, u), xs.at[s, j, u], xr.at[s, j, u], dev(c, f, k)
+            unit(source, j, u), unit(source, j, u), xs.at[s - 1, 0], xr.at[s - 1, j, u], dev(c, f, k)
         )
 
     units = [
@@ -163,13 +166,13 @@
             for s in range(1, chips):
                 goes(c, j, u, s, lambda: exchange(s, j, u).start())
             if route(u) in (None, 0):
-                pl.when(crosses(f, target(c, j)))(lambda: forward(c, j, u).start())
+                pl.when(crosses(f, target(c, j)))(lambda: forward(c, j, u, 0).start())
 
     load[2].wait()
     own_pair = c * 2 + k
     down_out[:, down_cols(own_pair)] = down[...].astype(jnp.bfloat16)
     down_half = down.shape[0] // 2
-    chunks = xds.shape[2]
+    chunks = xdr.shape[2]
     chunk = down_half // chunks
 
     def down_own(core):
@@ -189,17 +192,16 @@
     def down_across(s, position, i):
         held = down_piece(pair_of(c, position), k, i)
         return remote(
-            held, held, xds.at[s, position, i], xdr.at[s, position, i],
-            dev(lax.rem(c + s, chips), f, k),
-        )
-
-    def down_relay(s, position, i, core):
-        held = down_piece(pair_of(lax.rem(c + chips - s, chips), position), core, i)
-        return remote(held, held, pds.at[s, position, i], pdr.at[s, position, i], dev(c, f, 1 - k))
-
-    def down_arrival(s, position, i):
+            held, held, xds.at[0], xdr.at[s - 1, position, i], dev(lax.rem(c + s, chips), f, k)
+        )
+
+    def down_relay(s, position, i):
         held = down_piece(pair_of(lax.rem(c + chips - s, chips), position), k, i)
-        return remote(held, held, xds.at[s, position, i], xdr.at[s, position, i], dev(c, f, k))
+        return remote(held, held, pds.at[0], pdr.at[s - 1, position, i], dev(c, f, 1 - k))
+
+    def down_arrival(s, position, i, semaphore):
+        held = down_piece(0, k, i)
+        return remote(held, held, xds.at[0], semaphore.at[s - 1, position, i], dev(c, f, k))
 
     load[3].wait()
     widened = tokens[...].astype(jnp.float32)
@@ -210,58 +212,76 @@
 
     owner = f // (2 * blocks)
     offset = lax.rem(c + chips - owner, chips)
-    lone = single * piece
-
-    def alone(shard):
-        return jnp.logical_and(crosses(shard, f), offset < 2)
-
-    def lone_rows(shard):
-        return half_rows(shard, k, (1 - offset) * lone, lone)
-
-    def lone_arrival(shard):
+    lone = [count * piece for count in single]
+
+    def alone(shard, way):
+        return jnp.logical_and(crosses(shard, f), offset == way)
+
+    def lone_rows(shard, way):
+        return half_rows(shard, k, lone[1] if way == 0 else 0, lone[way])
+
+    def lone_arrival(shard, way):
+        held = lone_rows(shard, way)
+        return remote(held, held, msend.at[0], frecv.at[shards + shard], dev(c, f, k))
+
+    def lone_relay(shard, way, s):
+        held = lone_rows(shard, way)
         return remote(
-            lone_rows(shard), lone_rows(shard), msend.at[shard, 0], frecv.at[shards + shard], dev(c, f, k)
-        )
-
-    def lone_relay(shard, s):
-        return remote(
-            lone_rows(shard), lone_rows(shard), msend.at[shard, s], frecv.at[shard],
-            dev(lax.rem(c + s, chips), f, k),
-        )
-
+            held, held, msend.at[0], frecv.at[shard], dev(lax.rem(c + s, chips), f, k)
+        )
+
+    ways = [way for way in range(2) if single[way]]
     even = not shards & (shards - 1)
-    far = [s for s in range(1, shards) if single and (not even or s & (shards // 2))]
+    far = [s for s in range(1, shards) if sum(single) and (not even or s & (shards // 2))]
 
     def relay_lone():
         for step in far:
             shard = flipped(f, step, shards)
 
-            @pl.when(alone(shard))
+            for way in ways:
+                @pl.when(alone(shard, way))
+                def _():
+                    lone_arrival(shard, way).wait_recv()
+                    for s in range(1, chips):
+                        lone_relay(shard, way, s).start()
+
+    order_down = [(position, i) for position in range(2) for i in range(chunks)]
+
+    def send_down(pieces_of):
+        for position, i in pieces_of:
+            for s in range(1, chips):
+                down_across(s, position, i).start()
+
+    early = crosses(f, target(c, 0))
+
+    @pl.when(early)
+    def _():
+        down_own(1 - k).wait_recv()
+        send_down(order_down[:1])
+
+    for q, group in enumerate(units):
+        if q == max(0, slices - 1):
+            @pl.when(early)
             def _():
-                lone_arrival(shard).wait_recv()
-                for s in range(1, chips):
-                    lone_relay(shard, s).start()
-
-    def send_down():
-        down_own(1 - k).wait_recv()
-        for position in range(2):
-            for i in range(chunks):
-                for s in range(1, chips):
-                    down_across(s, position, i).start()
-
-    for q, group in enumerate(units):
+                relay_lone()
+                send_down(order_down[1:])
+
         for j, u in group:
-            when_not(crosses(f, target(c, j)))(lambda: start_forward(c, j, u))
+            when_not(crosses(f, target(c, j)))(lambda: start_forward(c, j, u, 0))
             for s in range(1, chips):
                 source = lax.rem(c + chips - s, chips)
 
                 def pass_on():
                     exchanged(s, j, u).wait_recv()
-                    start_forward(source, j, u)
+                    start_forward(source, j, u, s)
 
                 goes(source, j, u, s, pass_on)
-    relay_lone()
-    send_down()
+
+    @when_not(early)
+    def _():
+        relay_lone()
+        down_own(1 - k).wait_recv()
+        send_down(order_down)
 
     source_core = lax.rem(f // blocks, 2)
     own_stays = source_core == k
@@ -269,16 +289,14 @@
     def arrive(shard, step):
         def arrival(count):
             held = half_rows(shard, k, 0, count)
-            return remote(held, held, ps.at[shard], frecv.at[shard], dev(c, f, 1 - k))
+            return remote(held, held, ps.at[0], frecv.at[shard], dev(c, f, 1 - k))
 
         if step in far:
-            @pl.when(alone(shard))
-            def _():
-                arrival(half - lone).wait_recv()
-
-            @when_not(alone(shard))
-            def _():
-                arrival(half).wait_recv()
+            whole = jnp.logical_not(crosses(shard, f))
+            for way in ways:
+                pl.when(alone(shard, way))(lambda: arrival(half - lone[way]).wait_recv())
+            rest = jnp.logical_or(whole, functools.reduce(jnp.logical_and, [offset != way for way in ways]))
+            pl.when(rest)(lambda: arrival(half).wait_recv())
         elif step == 0:
             @when_not(own_stays)
             def _():
@@ -288,7 +306,7 @@
 
     def relay(shard, core):
         held = half_rows(shard, core)
-        return remote(held, held, ps.at[shard], pr.at[shard], dev(c, f, 1 - k))
+        return remote(held, held, ps.at[0], pr.at[shard], dev(c, f, 1 - k))
 
     def accumulate(shard, first):
         weights = up_out[pl.ds(pl.multiple_of(shard * rows, rows), rows), :]
@@ -312,27 +330,30 @@
     accumulate(order[-1], False)
     hidden[...] = jnp.square(jnp.maximum(acc[...], 0.0)).astype(jnp.bfloat16)
 
-    pieces = ys.shape[1]
+    pieces = yr.shape[1]
     span = mixed.shape[0] // pieces
 
+    def place(i):
+        return pl.ds(i * span, span)
+
     def across(pair, i):
-        at = pl.ds(i * span, span)
+        at = place(i)
         return remote(
-            part.at[2 * pair + 1 - y, at], ybuf.at[pair, at], ys.at[pair, i], yr.at[pair, i],
+            part.at[2 * pair + 1 - y, at], ybuf.at[pair, at], ys.at[0], yr.at[pair, i],
             dev(c, z * 2 + 1 - y, k),
         )
 
     def along(pair, i):
-        at = pl.ds(i * span, span)
+        at = place(i)
         to = z + jnp.where(pair > z, 1, -1)
         slot = jnp.where(jnp.logical_and(pair < z, pair == to), pairs, pair)
         return remote(
-            zout.at[pair, at], zin.at[slot, at], zs.at[pair, i], zr.at[slot, i], dev(c, to * 2 + y, k)
+            zout.at[pair, at], zin.at[slot, at], zs.at[0], zr.at[slot, i], dev(c, to * 2 + y, k)
         )
 
     def carried(slot, i):
-        held = zin.at[slot, pl.ds(i * span, span)]
-        return remote(held, held, zs.at[0, i], zr.at[slot, i], dev(c, f, k))
+        held = zin.at[slot, place(i)]
+        return remote(held, held, zs.at[0], zr.at[slot, i], dev(c, f, k))
 
     def multiply(pair):
         both = jnp.dot(
@@ -347,7 +368,7 @@
         inner = jnp.logical_and(pair != z, jnp.where(pair > z, z > 0, z < pairs - 1))
         outer = jnp.logical_and(pair != z, jnp.logical_not(inner))
         for i in range(pieces):
-            at = pl.ds(i * span, span)
+            at = place(i)
 
             def wide_of(ref, slot):
                 return ref[slot, at].astype(jnp.float32)
@@ -389,60 +410,109 @@
 
     def fetch(s, position):
         for i in range(chunks):
-            down_arrival(s, position, i).wait_recv()
-            down_relay(s, position, i, k).start()
+            down_arrival(s, position, i, xdr).wait_recv()
+            down_relay(s, position, i).start()
         for i in range(chunks):
-            down_relay(s, position, i, 1 - k).wait_recv()
+            down_arrival(s, position, i, pdr).wait_recv()
 
     def pair_at(index):
         return pair_of(lax.rem(c + chips - index // 2, chips), lax.rem(index, 2))
 
     last = 2 * lax.rem(z // 2 + chips - c, chips) + 1
-    sequence = [pair_at(i + jnp.where(i < last, 0, 1)) for i in range(pairs - 1)] + [pair_at(last)]
-    for i in range(pairs):
-        if i > 1:
-            fetch(i // 2, i % 2)
-        multiply(pair_at(i))
-        if i >= AHEAD:
-            reduce(sequence[i - AHEAD])
-    for pair in sequence[pairs - AHEAD:]:
-        reduce(pair)
-
-    down_own(k).wait_send()
-    for s in range(1, chips):
-        for position in range(2):
-            for i in range(chunks):
-                down_across(s, position, i).wait_send()
-                down_relay(s, position, i, k).wait_send()
-    for step in far:
-        shard = flipped(f, step, shards)
-
-        @pl.when(alone(shard))
+    home = last == 1
+
+    def index_at(i):
+        return last if i == pairs - 1 else i + jnp.where(i < last, 0, 1)
+
+    sequence = [pair_at(index_at(i)) for i in range(pairs)]
+
+    def take(i):
+        if i > 0:
+            index = index_at(i)
+            pl.when(index > 1)(lambda: fetch(index // 2, lax.rem(index, 2)))
+        multiply(sequence[i])
+
+    def sent(source, semaphore):
+        remote(source, source, semaphore, xr.at[0, 0, 0], dev(c, f, k)).wait_send()
+
+    def gathered():
+        down_own(k).wait_send()
+        for way in ways:
+            passed = (chips - 1) * (shards // 2) * lone[way]
+            pl.when(offset == way)(lambda: sent(up_out.at[pl.ds(0, passed), :], msend.at[0]))
+        sent(up_out.at[pl.ds(0, shards * half), :], ps.at[0])
+        for s in range(chips):
+            source = lax.rem(c + chips - s, chips)
+            count = [piece * sum(pinned(u, s) == which for u in range(2 * slices)) for which in range(2)]
+            for which in range(2):
+                if not count[which]:
+                    continue
+                if s > 0:
+                    def crossed():
+                        sent(gath.at[0, pl.ds(0, count[which]), :], xs.at[s - 1, which])
+
+                    if which:
+                        when_not(crosses(f, target(c, 0)))(crossed)
+                    else:
+                        crossed()
+                for j in range(blocks):
+                    to = target(source, j)
+
+                    def left(rows_left):
+                        sent(gath.at[0, pl.ds(0, rows_left), pl.ds(0, block)], fsend.at[s, j, which])
+
+                    gone = jnp.logical_not(crosses(f, to)) if which else to >= 0
+                    pl.when(jnp.logical_and(gone, to != f))(lambda: left(count[which]))
+                    pl.when(to == f)(lambda: left(count[which] // 2))
+
+    def run(*events):
+        for action, i in events:
+            (take if action == "take" else settle)(i)
+
+    def settle(i):
+        reduce(sequence[i])
+
+    outer = jnp.logical_or(z == 0, z == pairs - 1)
+    own = pairs - 1
+    takes = [("take", i) for i in range(2, own)]
+    take(0)
+    take(1)
+    gathered()
+
+    @pl.when(jnp.logical_and(home, outer))
+    def _():
+        run(("settle", 0), *takes, ("take", own))
+
+    @pl.when(jnp.logical_and(home, jnp.logical_not(outer)))
+    def _():
+        run(*takes, ("take", own), ("settle", 0))
+
+    @when_not(home)
+    def _():
+        run(*takes, ("settle", 0))
+
+        @pl.when(outer)
         def _():
-            for s in range(1, chips):
-                lone_relay(shard, s).wait_send()
-    for group in units:
-        for j, u in group:
-            for s in range(1, chips):
-                goes(c, j, u, s, lambda: exchange(s, j, u).wait_send())
-            for s in range(chips):
-                source = lax.rem(c + chips - s, chips)
-
-                def sent():
-                    @when_not(stays(source, j, u))
-                    def _():
-                        forward(source, j, u).wait_send()
-
-                goes(source, j, u, s, sent)
-    for shard in order:
-        relay(shard, k).wait_send()
-    for pair in sequence:
-        for i in range(pieces):
-            across(pair, i).wait_send()
-
-            @pl.when(pair != z)
-            def _():
-                along(pair, i).wait_send()
+            settle(1)
+
+        take(own)
+
+        @when_not(outer)
+        def _():
+            settle(1)
+
+    @pl.when(home)
+    def _():
+        settle(1)
+
+    for i in range(2, pairs):
+        settle(i)
+
+    crossed = down_out.at[pl.ds(0, down_half), pl.ds(0, 2 * (chips - 1) * cols)]
+    sent(crossed, xds.at[0])
+    sent(crossed, pds.at[0])
+    sent(part.at[pl.ds(0, pairs)], ys.at[0])
+    sent(zout.at[pl.ds(0, pairs - 1)], zs.at[0])
 
 
 def copy_kernel(up, down, mixed, up_out, down_out, mixed_out, sems):
@@ -465,14 +535,15 @@
     group = gr * tp
     chips = group // 2
     slices = max(1, rows // 2 // SLICE_ROWS)
-    single = slices * SINGLE_NUM // SINGLE_DEN if chips > 1 else 0
+    single = [slices * some // of if chips > 1 else 0 for some, of in SINGLE]
     block = width * group // fs
     blocks = width // block
     count, depth = tokens.shape
     model = cols * group
     pairs = fs // 2
     wide = model // fs
-    assert pairs == group and pairs > 1
+    assert pairs == group and pairs > 2 and pairs % blocks == 0
+    others = max(1, chips - 1)
     vmem = pl.BlockSpec(memory_space=pltpu.VMEM)
     hbm = pl.BlockSpec(memory_space=pltpu.HBM)
     bf16, f32 = jnp.bfloat16, jnp.float32
@@ -501,10 +572,10 @@
             pltpu.VMEM((pairs, count, wide), bf16),
             pltpu.VMEM((pairs, count, wide), bf16),
             pltpu.VMEM((pairs + 1, count, wide), bf16),
-            *[dma((chips, blocks, 2 * slices)) for _ in range(3)], dma((2 * fs,)), dma((fs, chips)),
-            dma((fs,)), dma((fs,)), dma((1,)), dma((1,)),
-            *[dma((chips, 2, DOWN_CHUNKS)) for _ in range(4)],
-            *[dma((pairs, PIECES)) for _ in range(3)], dma((pairs + 1, PIECES)),
+            dma((others, 2)), dma((others, blocks, 2 * slices)), dma((chips, blocks, 2)), dma((2 * fs,)),
+            dma((1,)), dma((1,)), dma((fs,)), dma((1,)), dma((1,)),
+            dma((1,)), dma((others, 2, DOWN_CHUNKS)), dma((1,)), dma((others, 2, DOWN_CHUNKS)),
+            dma((1,)), dma((pairs, PIECES)), dma((1,)), dma((pairs + 1, PIECES)),
         ],
         compiler_params=pltpu.CompilerParams(
             collective_id=0, has_side_effects=True, vmem_limit_bytes=FUSED_VMEM * MIB

time: 82.8 us -> 78.2 us (0.944)
  Pallas kernels: 81.7 us -> 77.3 us
    pallas_call x1, Pallas kernels: 78.2 us -> 73.9 us  [per_device(): pl.pallas_call(functools.partial(fused_kernel, tp, blocks, fs, single), o...]
where the time goes in v3:
time: 78.2 us; the launch traced here: 78 us
  Pallas kernels  77.3 us (99%)
    pallas_call x1, Pallas kernels, per_device(): pl.pallas_call(functools.partial(fused_kernel, tp, blocks, fs, single), o...  73.9 us
    pallas_call x1, Pallas kernels, per_device(): pl.pallas_call(copy_kernel, out_shape=results, in_specs=[vmem] * 3, out_s...  3.39 us

profile of v3, /device:TPU:10, one launch (start us, length us, event | category | flops | bytes accessed | tf_op | source)
XLA Modules:
  0.0 78.0 jit_solution(6435838971608278844)
XLA Ops:
  0.6 73.9 %shard_map.67 = (bf16[2048,1024]{1,0:T(8,128)(2,1)S(1)}, bf16[1024,2048]{1,0:T(8,128)(2,1)S(1)}, bf16[512,256]{1,0:T(8,128)(2,1)S(1)}) custom-call(bf16[512,2048]{1,0:T(8,128)(2,1)} %tokens_in.1, f32[1,256]{1,0:T(1,128)} %bitcast.1, f32[256,2048]{1,0:T(8,128)} %up_in.1, f32[1024,512]{1,0:T(8,128)} %down_in.1), custom_call_target="tpu_custom_call" | custom-call | flops 4294967296 | bytes 167772160 | tf_op jit(solution)/shard_map/pallas_call | solution.py:556
  74.6 3.4 %shard_map.68 = (bf16[2048,1024]{1,0:T(8,128)(2,1)}, bf16[1024,2048]{1,0:T(8,128)(2,1)}, bf16[512,256]{1,0:T(8,128)(2,1)}) custom-call(bf16[2048,1024]{1,0:T(8,128)(2,1)S(1)} %get-tuple-element.6.up, bf16[1024,2048]{1,0:T(8,128)(2,1)S(1)} %get-tuple-element.7.down, bf16[512,256]{1,0:T(8,128)(2,1)S(1)} %get-tuple-element.8.mixed), custom_call_target="tpu_custom_call" | custom-call | flops 131072 | bytes 18874368 | tf_op jit(solution)/shard_map/pallas_call | solution.py:587

commit v4 on v3

--- a/solution.py
+++ b/solution.py
@@ -16,6 +16,8 @@
 PIECES = 4
 DOWN_CHUNKS = 2
 COPY_CHUNKS = 2
+EARLY_SUMS = (1, 2)
+LATE_SUMS = 3
 
 
 def flipped(index, step, count):
@@ -364,10 +366,10 @@
         for i in range(pieces):
             across(pair, i).start()
 
-    def reduce(pair):
+    def reduce(pair, some):
         inner = jnp.logical_and(pair != z, jnp.where(pair > z, z > 0, z < pairs - 1))
         outer = jnp.logical_and(pair != z, jnp.logical_not(inner))
-        for i in range(pieces):
+        for i in some:
             at = place(i)
 
             def wide_of(ref, slot):
@@ -412,6 +414,8 @@
         for i in range(chunks):
             down_arrival(s, position, i, xdr).wait_recv()
             down_relay(s, position, i).start()
+
+    def fetched(s, position):
         for i in range(chunks):
             down_arrival(s, position, i, pdr).wait_recv()
 
@@ -426,11 +430,21 @@
 
     sequence = [pair_at(index_at(i)) for i in range(pairs)]
 
+    def begin(i):
+        index = index_at(i)
+        pl.when(index > 1)(lambda: fetch(index // 2, lax.rem(index, 2)))
+
+    def complete(i):
+        index = index_at(i)
+        pl.when(index > 1)(lambda: fetched(index // 2, lax.rem(index, 2)))
+        multiply(sequence[i])
+
     def take(i):
         if i > 0:
-            index = index_at(i)
-            pl.when(index > 1)(lambda: fetch(index // 2, lax.rem(index, 2)))
-        multiply(sequence[i])
+            begin(i)
+            complete(i)
+        else:
+            multiply(sequence[i])
 
     def sent(source, semaphore):
         remote(source, source, semaphore, xr.at[0, 0, 0], dev(c, f, k)).wait_send()
@@ -465,48 +479,59 @@
                     pl.when(jnp.logical_and(gone, to != f))(lambda: left(count[which]))
                     pl.when(to == f)(lambda: left(count[which] // 2))
 
-    def run(*events):
-        for action, i in events:
-            (take if action == "take" else settle)(i)
-
-    def settle(i):
-        reduce(sequence[i])
+    def settle(i, first=0, end=pieces):
+        reduce(sequence[i], range(first, end))
 
     outer = jnp.logical_or(z == 0, z == pairs - 1)
     own = pairs - 1
-    takes = [("take", i) for i in range(2, own)]
     take(0)
     take(1)
     gathered()
 
     @pl.when(jnp.logical_and(home, outer))
     def _():
-        run(("settle", 0), *takes, ("take", own))
+        settle(0)
+        for i in range(2, own):
+            settle(i - 1, 0, EARLY_SUMS[0])
+            begin(i)
+            settle(i - 1, EARLY_SUMS[0], EARLY_SUMS[1])
+            complete(i)
+            settle(i - 1, EARLY_SUMS[1], pieces)
+        take(own)
 
     @pl.when(jnp.logical_and(home, jnp.logical_not(outer)))
     def _():
-        run(*takes, ("take", own), ("settle", 0))
+        for i in range(2, pairs):
+            take(i)
+        if own == 3:
+            for n in range(pieces):
+                settle(0, n, n + 1)
+                settle(1, n, n + 1)
+        else:
+            for i in range(own - 1):
+                settle(i)
 
     @when_not(home)
     def _():
-        run(*takes, ("settle", 0))
+        for i in range(2, own):
+            take(i)
+        settle(0)
 
         @pl.when(outer)
         def _():
-            settle(1)
-
-        take(own)
-
-        @when_not(outer)
-        def _():
-            settle(1)
-
-    @pl.when(home)
-    def _():
-        settle(1)
-
-    for i in range(2, pairs):
-        settle(i)
+            settle(1, 0, LATE_SUMS)
+            begin(own)
+            settle(1, LATE_SUMS, pieces)
+
+        when_not(outer)(lambda: begin(own))
+        complete(own)
+        when_not(outer)(lambda: settle(1))
+
+        for i in range(2, own - 1):
+            settle(i)
+
+    settle(own - 1)
+    settle(own)
 
     crossed = down_out.at[pl.ds(0, down_half), pl.ds(0, 2 * (chips - 1) * cols)]
     sent(crossed, xds.at[0])

time: 78.2 us -> 75.9 us (0.971)
  the two profiles are of different devices: /device:TPU:10 before, /device:TPU:3 now
where the time goes in v4:
time: 75.9 us; the launch traced here: 75.7 us
  Pallas kernels  75 us (99%)
    pallas_call x1, Pallas kernels, per_device(): pl.pallas_call(functools.partial(fused_kernel, tp, blocks, fs, single), o...  71.7 us
    pallas_call x1, Pallas kernels, per_device(): pl.pallas_call(copy_kernel, out_shape=results, in_specs=[vmem] * 3, out_s...  3.39 us

profile of v4, /device:TPU:3, one launch (start us, length us, event | category | flops | bytes accessed | tf_op | source)
XLA Modules:
  0.0 75.7 jit_solution(2471747399304919215)
XLA Ops:
  0.6 71.7 %shard_map.67 = (bf16[2048,1024]{1,0:T(8,128)(2,1)S(1)}, bf16[1024,2048]{1,0:T(8,128)(2,1)S(1)}, bf16[512,256]{1,0:T(8,128)(2,1)S(1)}) custom-call(bf16[512,2048]{1,0:T(8,128)(2,1)} %tokens_in.1, f32[1,256]{1,0:T(1,128)} %bitcast.1, f32[256,2048]{1,0:T(8,128)} %up_in.1, f32[1024,512]{1,0:T(8,128)} %down_in.1), custom_call_target="tpu_custom_call" | custom-call | flops 4294967296 | bytes 167772160 | tf_op jit(solution)/shard_map/pallas_call | solution.py:581
  72.3 3.4 %shard_map.68 = (bf16[2048,1024]{1,0:T(8,128)(2,1)}, bf16[1024,2048]{1,0:T(8,128)(2,1)}, bf16[512,256]{1,0:T(8,128)(2,1)}) custom-call(bf16[2048,1024]{1,0:T(8,128)(2,1)S(1)} %get-tuple-element.6.up, bf16[1024,2048]{1,0:T(8,128)(2,1)S(1)} %get-tuple-element.7.down, bf16[512,256]{1,0:T(8,128)(2,1)S(1)} %get-tuple-element.8.mixed), custom_call_target="tpu_custom_call" | custom-call | flops 131072 | bytes 18874368 | tf_op jit(solution)/shard_map/pallas_call | solution.py:612

commit v5 on v4

--- a/solution.py
+++ b/solution.py
@@ -329,8 +329,6 @@
             relay(before, 1 - k).wait_recv()
             accumulate(before, position == 1)
     relay(order[-1], 1 - k).wait_recv()
-    accumulate(order[-1], False)
-    hidden[...] = jnp.square(jnp.maximum(acc[...], 0.0)).astype(jnp.bfloat16)
 
     pieces = yr.shape[1]
     span = mixed.shape[0] // pieces
@@ -357,13 +355,15 @@
         held = zin.at[slot, place(i)]
         return remote(held, held, zs.at[0], zr.at[slot, i], dev(c, f, k))
 
-    def multiply(pair):
+    def multiply(pair, first=0, end=None):
+        end = pieces if end is None else end
+        at = pl.ds(first * span, (end - first) * span)
         both = jnp.dot(
-            hidden[...], down_out[:, down_cols(pair)], preferred_element_type=jnp.float32
+            hidden[at], down_out[:, down_cols(pair)], preferred_element_type=jnp.float32
         ).astype(jnp.bfloat16)
-        part[2 * pair] = both[:, :wide]
-        part[2 * pair + 1] = both[:, wide:]
-        for i in range(pieces):
+        part[2 * pair, at] = both[:, :wide]
+        part[2 * pair + 1, at] = both[:, wide:]
+        for i in range(first, end):
             across(pair, i).start()
 
     def reduce(pair, some):
@@ -484,7 +484,13 @@
 
     outer = jnp.logical_or(z == 0, z == pairs - 1)
     own = pairs - 1
-    take(0)
+    final = up_out.at[pl.ds(pl.multiple_of(order[-1] * rows, rows), rows), :]
+    for first in range(0, pieces, pieces // 2):
+        end = first + pieces // 2
+        at = pl.ds(first * span, (end - first) * span)
+        product = jnp.dot(normed[order[-1], at], final[...], preferred_element_type=jnp.float32)
+        hidden[at] = jnp.square(jnp.maximum(acc[at] + product, 0.0)).astype(jnp.bfloat16)
+        multiply(sequence[0], first, end)
     take(1)
     gathered()
 

time: 75.9 us -> 75.4 us (level)
  no operation moved by 1% of the time
where the time goes in v5:
time: 75.4 us; the launch traced here: 75.2 us
  Pallas kernels  74.6 us (99%)
    pallas_call x1, Pallas kernels, per_device(): pl.pallas_call(functools.partial(fused_kernel, tp, blocks, fs, single), o...  71.2 us
    pallas_call x1, Pallas kernels, per_device(): pl.pallas_call(copy_kernel, out_shape=results, in_specs=[vmem] * 3, out_s...  3.39 us

profile of v5, /device:TPU:3, one launch (start us, length us, event | category | flops | bytes accessed | tf_op | source)
XLA Modules:
  0.0 75.2 jit_solution(2818376722116399000)
XLA Ops:
  0.6 71.2 %shard_map.67 = (bf16[2048,1024]{1,0:T(8,128)(2,1)S(1)}, bf16[1024,2048]{1,0:T(8,128)(2,1)S(1)}, bf16[512,256]{1,0:T(8,128)(2,1)S(1)}) custom-call(bf16[512,2048]{1,0:T(8,128)(2,1)} %tokens_in.1, f32[1,256]{1,0:T(1,128)} %bitcast.1, f32[256,2048]{1,0:T(8,128)} %up_in.1, f32[1024,512]{1,0:T(8,128)} %down_in.1), custom_call_target="tpu_custom_call" | custom-call | flops 4294967296 | bytes 167772160 | tf_op jit(solution)/shard_map/pallas_call | solution.py:587
  71.8 3.4 %shard_map.68 = (bf16[2048,1024]{1,0:T(8,128)(2,1)}, bf16[1024,2048]{1,0:T(8,128)(2,1)}, bf16[512,256]{1,0:T(8,128)(2,1)}) custom-call(bf16[2048,1024]{1,0:T(8,128)(2,1)S(1)} %get-tuple-element.6.up, bf16[1024,2048]{1,0:T(8,128)(2,1)S(1)} %get-tuple-element.7.down, bf16[512,256]{1,0:T(8,128)(2,1)S(1)} %get-tuple-element.8.mixed), custom_call_target="tpu_custom_call" | custom-call | flops 131072 | bytes 18874368 | tf_op jit(solution)/shard_map/pallas_call | solution.py:618
